TPU v7x, 32 devices: a whole 2x2x4 slice. The times are simulated.
32 devices in a mesh: grp: 2 (over x), ep: 16 (over z, y, core).
Axes of the slice: x: 2, y: 2, z: 4, core: 2. Of those that a mesh axis runs over, the one named last changes fastest.
Arguments:
- sequence_input_rows: bfloat16 [224, 2048], P(('grp', 'ep')), parts along dimension 0, may hold values from -6 to 6
- value_key_state: float32 [224, 32, 64, 64], P(('grp', 'ep')), parts along dimension 0, may hold values from -4 to 4
- receptance_matrix: bfloat16 [2048, 2048], P(None, 'ep'), may hold values from -0.125 to 0.125
- key_matrix: bfloat16 [2048, 2048], P(None, 'ep'), may hold values from -0.125 to 0.125
- value_matrix: bfloat16 [2048, 2048], P(None, 'ep'), may hold values from -0.125 to 0.125
- decay_lowrank_input: bfloat16 [2048, 64], replicated, may hold values from -0.125 to 0.125
- decay_lowrank_output: bfloat16 [64, 2048], replicated, may hold values from -0.75 to 0.75
- decay_base_preact: float32 [2048], replicated, may hold values from -6 to -1
- context_rate_input: bfloat16 [2048, 64], replicated, may hold values from -0.125 to 0.125
- context_rate_output: bfloat16 [64, 2048], replicated, may hold values from -0.75 to 0.75
- context_rate_base: float32 [2048], replicated, may hold values from -4 to 4
- removal_key_scale: float32 [2048], replicated, may hold values from 0.1 to 1.9
- key_context_rate_blend: float32 [2048], replicated, may hold values from 0.1 to 1.9
- present_item_coefficient: float32 [32, 64], replicated, may hold values from -0.9 to 0.9
- head_norm_gain: float32 [2048], replicated, may hold values from 0.1 to 1.9
- mixer_output_matrix: bfloat16 [2048, 2048], P(None, 'ep'), may hold values from -0.125 to 0.125
- mixer_norm_gain: float32 [2048], replicated, may hold values from 0.1 to 1.9
- group_router_columns: bfloat16 [2048, 4], replicated, may hold values from -8 to 8
- expert_router_columns: bfloat16 [2048, 16], replicated, may hold values from -0.125 to 0.125
- expert_gate_matrix: bfloat16 [16, 2048, 256], P('ep'), may hold values from -0.125 to 0.125
- expert_up_matrix: bfloat16 [16, 2048, 256], P('ep'), may hold values from -0.125 to 0.125
- expert_down_matrix: bfloat16 [16, 256, 2048], P('ep'), may hold values from -0.375 to 0.375
- final_norm_gain: float32 [2048], replicated, may hold values from 0.1 to 1.9
- routes: int32 [224, 4], P(('grp', 'ep')), parts along dimension 0, may hold values from 0 to 15, as said below
Outputs:
- tokens_out: bfloat16 [224, 2048], P(('grp', 'ep')), parts along dimension 0
- next_recurrent_state: float32 [224, 32, 64, 64], P(('grp', 'ep')), parts along dimension 0
There are 2 independent parts, one for each index of `grp`. A program takes and returns all parts, laid end to end along the dimension named above; an argument that names none is the same for every part. Nothing has to cross between parts.
Inputs may be any that keep to these rules, and one draw needn't show every extreme that they name: `routes`: the 4 experts of a row are different and lie in the same group (expert // 4). In each aligned block of 7 rows (the rows of one device) no expert is named more than 2 times, and in every block some expert is named exactly 2 times.
All inputs are finite; a program needn't handle non-finite values.
Results may differ from a plain program's by a relative error of at most 0.0067.
Values may be sent and summed in bfloat16 or wider, within the bound.
A program may use at most 128 MiB of HBM per device.

v0:
```python
import jax
import jax.numpy as jnp
from jax import lax
from jax.sharding import PartitionSpec as P

CAP = 2
residual_scale = 8.0**0.25
norm_eps = 1e-05
group_eps = 0.00064


def layer_norm(values, norm_gain):
    center = jnp.mean(values, -1, keepdims=True)
    spread = jnp.mean(jnp.square(values - center), -1, keepdims=True)
    return (values - center) * lax.rsqrt(spread + norm_eps) * norm_gain


def token_mixer_step(
    sequence_input_rows,
    receptance_rows,
    key_projected_rows,
    value_projected_rows,
    value_key_state,
    decay_lowrank_input,
    decay_lowrank_output,
    decay_base_preact,
    context_rate_input,
    context_rate_output,
    context_rate_base,
    removal_key_scale,
    key_context_rate_blend,
    present_item_coefficient,
    head_norm_gain,
):
    series_entry_number = sequence_input_rows.shape[0]
    attention_subspace_number, subspace_dimension = present_item_coefficient.shape
    decay_low = jnp.tanh(
        jnp.dot(sequence_input_rows, decay_lowrank_input, preferred_element_type=jnp.float32)
    ).astype(jnp.bfloat16)
    decay_pre = decay_base_preact + jnp.dot(
        decay_low, decay_lowrank_output, preferred_element_type=jnp.float32
    )
    log_rate = -jax.nn.softplus(-decay_pre) - 0.5
    decay = jnp.exp(-jnp.exp(log_rate))
    iclr_low = jnp.dot(
        sequence_input_rows, context_rate_input, preferred_element_type=jnp.float32
    ).astype(jnp.bfloat16)
    iclr_rate = jax.nn.sigmoid(
        context_rate_base
        + jnp.dot(iclr_low, context_rate_output, preferred_element_type=jnp.float32)
    )

    def to_heads(values):
        return values.astype(jnp.float32).reshape(
            series_entry_number, attention_subspace_number, subspace_dimension
        )

    acceptance_subspaces = to_heads(receptance_rows)
    key_heads = to_heads(key_projected_rows)
    content_subspace_entries = to_heads(value_projected_rows)
    decay_heads = to_heads(decay)
    rate_heads = to_heads(iclr_rate)
    scaled_key = key_heads * removal_key_scale.reshape(
        attention_subspace_number, subspace_dimension
    )
    removal_dir = scaled_key * lax.rsqrt(
        jnp.sum(scaled_key * scaled_key, -1, keepdims=True) + 1e-06
    )
    adjusted_lookup_vector = key_heads * (
        1.0
        + (rate_heads - 1.0)
        * key_context_rate_blend.reshape(attention_subspace_number, subspace_dimension)
    )
    removed = jnp.einsum(
        "bhvk,bhk->bhv", value_key_state, removal_dir, precision=lax.Precision.HIGHEST
    )
    next_recurrent_state = (
        value_key_state * decay_heads[:, :, None, :]
        - removed[..., None] * (removal_dir * rate_heads)[:, :, None, :]
        + content_subspace_entries[..., None] * adjusted_lookup_vector[:, :, None, :]
    )
    readout = jnp.einsum(
        "bhvk,bhk->bhv", next_recurrent_state, acceptance_subspaces, precision=lax.Precision.HIGHEST
    )
    center = jnp.mean(readout, -1, keepdims=True)
    spread = jnp.mean(jnp.square(readout - center), -1, keepdims=True)
    standardized_entries = (
        (readout - center)
        * lax.rsqrt(spread + group_eps)
        * head_norm_gain.reshape(attention_subspace_number, subspace_dimension)
    )
    present_extra_reward = (
        jnp.sum(
            acceptance_subspaces * adjusted_lookup_vector * present_item_coefficient,
            -1,
            keepdims=True,
        )
        * content_subspace_entries
    )
    attention_mixing_outcome = (
        (standardized_entries + present_extra_reward)
        .reshape(series_entry_number, attention_subspace_number * subspace_dimension)
        .astype(jnp.bfloat16)
    )
    return (attention_mixing_outcome, next_recurrent_state)


def routing_gate(hidden, route_rows, chosen, group_router_columns, expert_router_columns):
    group_count = group_router_columns.shape[1]
    expert_count = expert_router_columns.shape[1]
    per_group = expert_count // group_count
    group_logits = jnp.dot(hidden, group_router_columns, preferred_element_type=jnp.float32)
    expert_logits = jnp.dot(hidden, expert_router_columns, preferred_element_type=jnp.float32)
    largest = jnp.max(group_logits, -1, keepdims=True)
    lifted = jnp.exp(group_logits - largest)
    in_group = (chosen // per_group)[:, None] == jnp.arange(group_count, dtype=jnp.int32)[None, :]
    group_prob = jnp.sum(jnp.where(in_group, lifted, 0.0), -1) / jnp.sum(lifted, -1)
    columns = jnp.arange(expert_count, dtype=jnp.int32)[None, :]
    chosen_logit = jnp.sum(jnp.where(chosen[:, None] == columns, expert_logits, 0.0), -1)
    total = jnp.zeros_like(chosen_logit)
    for slot in range(route_rows.shape[1]):
        other_logit = jnp.sum(
            jnp.where(route_rows[:, slot][:, None] == columns, expert_logits, 0.0), -1
        )
        total = total + jnp.exp(other_logit - chosen_logit)
    return group_prob / total


def expert_mlp(inputs, expert_weights):
    gate_weight, up_weight, down_weight = expert_weights
    gate_part = jnp.dot(inputs, gate_weight[0], preferred_element_type=jnp.float32)
    up_part = jnp.dot(inputs, up_weight[0], preferred_element_type=jnp.float32)
    act = (jax.nn.silu(gate_part) * up_part).astype(jnp.bfloat16)
    return jnp.dot(act, down_weight[0], preferred_element_type=jnp.float32).astype(jnp.bfloat16)


def by_exchange(hidden, routes, routers, expert_weights):
    series_entry_number, model_width = hidden.shape
    expert_count = routers[1].shape[1]
    is_named = routes[:, :, None] == jnp.arange(expert_count, dtype=jnp.int32)[None, None, :]
    per_row = jnp.sum(is_named.astype(jnp.int32), 1)
    before = jnp.cumsum(per_row, 0) - per_row
    slot_rank = jnp.sum(jnp.where(is_named, before[:, None, :], 0), -1)
    slot_index = routes * CAP + slot_rank
    placing = (
        slot_index[:, :, None] == jnp.arange(expert_count * CAP, dtype=jnp.int32)[None, None, :]
    ).astype(jnp.bfloat16)
    outgoing = jnp.einsum("rks,rd->sd", placing, hidden, preferred_element_type=jnp.float32)
    outgoing = outgoing.astype(jnp.bfloat16).reshape(expert_count, CAP, model_width)
    incoming = lax.all_to_all(outgoing, "ep", split_axis=0, concat_axis=0, tiled=True)
    flat_rows = incoming.reshape(-1, model_width)
    finished = expert_mlp(flat_rows, expert_weights).reshape(incoming.shape)
    returned = lax.all_to_all(finished, "ep", split_axis=0, concat_axis=0, tiled=True).reshape(
        expert_count * CAP, model_width
    )
    gate_values = jnp.stack(
        [
            routing_gate(hidden, routes, routes[:, slot], routers[0], routers[1])
            for slot in range(routes.shape[1])
        ],
        1,
    )
    picked = returned[slot_index]
    return jnp.sum(gate_values[:, :, None] * picked.astype(jnp.float32), 1)


def on_device(
    sequence_input_rows,
    value_key_state,
    receptance_matrix,
    key_matrix,
    value_matrix,
    decay_lowrank_input,
    decay_lowrank_output,
    decay_base_preact,
    context_rate_input,
    context_rate_output,
    context_rate_base,
    removal_key_scale,
    key_context_rate_blend,
    present_item_coefficient,
    head_norm_gain,
    mixer_output_matrix,
    mixer_norm_gain,
    group_router_columns,
    expert_router_columns,
    expert_gate_matrix,
    expert_up_matrix,
    expert_down_matrix,
    final_norm_gain,
    routes,
):
    section = lax.all_gather(sequence_input_rows, "ep", axis=0, tiled=True)
    columns = [
        jnp.dot(section, weight, preferred_element_type=jnp.float32).astype(jnp.bfloat16)
        for weight in (receptance_matrix, key_matrix, value_matrix)
    ]
    projected = jnp.stack(columns, axis=1)
    own_heads = lax.all_to_all(projected, "ep", split_axis=0, concat_axis=2, tiled=True)
    attention_mixing_outcome, next_recurrent_state = token_mixer_step(
        sequence_input_rows,
        own_heads[:, 0],
        own_heads[:, 1],
        own_heads[:, 2],
        value_key_state,
        decay_lowrank_input,
        decay_lowrank_output,
        decay_base_preact,
        context_rate_input,
        context_rate_output,
        context_rate_base,
        removal_key_scale,
        key_context_rate_blend,
        present_item_coefficient,
        head_norm_gain,
    )
    out_columns = jnp.dot(
        lax.all_gather(attention_mixing_outcome, "ep", axis=0, tiled=True),
        mixer_output_matrix,
        preferred_element_type=jnp.float32,
    ).astype(jnp.bfloat16)
    attn_out = lax.all_to_all(out_columns, "ep", split_axis=0, concat_axis=1, tiled=True)
    hidden = layer_norm(
        residual_scale * sequence_input_rows.astype(jnp.float32) + attn_out.astype(jnp.float32),
        mixer_norm_gain,
    ).astype(jnp.bfloat16)
    expert_weights = (expert_gate_matrix, expert_up_matrix, expert_down_matrix)
    routers = (group_router_columns, expert_router_columns)
    expert_sum = by_exchange(hidden, routes, routers, expert_weights)
    tokens_out = layer_norm(
        residual_scale * hidden.astype(jnp.float32) + expert_sum, final_norm_gain
    ).astype(jnp.bfloat16)
    return (tokens_out, next_recurrent_state)


def solution(mesh):
    in_specs = (
        P(("grp", "ep"), None),
        P(("grp", "ep"), None, None, None),
        P(None, "ep"),
        P(None, "ep"),
        P(None, "ep"),
        P(),
        P(),
        P(),
        P(),
        P(),
        P(),
        P(),
        P(),
        P(),
        P(),
        P(None, "ep"),
        P(),
        P(),
        P(),
        P("ep", None, None),
        P("ep", None, None),
        P("ep", None, None),
        P(),
        P(("grp", "ep"), None),
    )
    out_specs = (P(("grp", "ep"), None), P(("grp", "ep"), None, None, None))
    return jax.shard_map(
        on_device, mesh=mesh, in_specs=in_specs, out_specs=out_specs, check_vma=False
    )
```

profile of v0, /device:TPU:0, one launch (start us, length us, event | category | flops | bytes accessed | tf_op | source)
XLA Modules:
  0.0 138.3 jit_solution(8020242776843022416)
XLA Ops:
  0.6 25.0 %all-gather = bf16[16,7,2048]{2,1,0:T(8,128)(2,1)S(1)} all-gather(bf16[1,7,2048]{2,1,0:T(8,128)(2,1)} %bitcast.101), channel_id=1, replica_groups=mesh['grp'=2,'ep'=16] {'ep'}, dimensions={0}, use_global_device_ids=true | all-gather | bytes 487424 | tf_op jit(solution)/shard_map/all_gather | solution.py:193
  25.6 0.2 reshape.474
  25.8 1.3 fusion.10
  27.1 1.3 fusion.11
  28.4 1.3 fusion.9
  29.7 0.7 copy.40
  30.4 3.5 %all-to-all-start = ((bf16[112,3,128]{2,1,0:T(4,128)(2,1)}), bf16[112,3,128]{2,1,0:T(4,128)(2,1)S(1)}, u32[]{:S(2)}, u32[]{:S(2)}) async-start(bf16[112,3,128]{2,1,0:T(4,128)(2,1)} %copy.40), calls=%async_computation | async-start | bytes 229376 | tf_op jit(solution)/shard_map/all_to_all | solution.py:199
  34.0 0.8 copy.43
  34.7 0.1 convert_reduce_fusion.1
  34.9 0.3 select_reduce_fusion
  35.1 1.4 %fusion.4 = f32[7,2048]{1,0:T(8,128)S(1)} fusion(bf16[64,2048]{1,0:T(8,128)(2,1)} %param.33, bf16[7,2048]{1,0:T(8,128)(2,1)} %param.24, bf16[2048,64]{0,1:T(8,128)(2,1)} %param.32, f32[2048]{0:T(1024)} %param.34), kind=kOutput, calls=%fused_computation.9 | convolution fusion | flops 3727808 | bytes 618496 | tf_op jit(solution)/shard_map/dot_general | solution.py:50
  36.6 1.5 %fusion.24 = f32[7,2048]{1,0:T(8,128)S(1)} fusion(bf16[64,2048]{1,0:T(8,128)(2,1)} %param.30, bf16[7,2048]{1,0:T(8,128)(2,1)} %param.24, bf16[2048,64]{0,1:T(8,128)(2,1)} %param.29, f32[2048]{0:T(1024)} %param.31), kind=kOutput, calls=%fused_computation.45 | convolution fusion | flops 3828160 | bytes 618496 | tf_op jit(solution)/shard_map/dot_general | solution.py:40
  38.1 0.8 slice_bitcast_fusion.2
  38.9 0.8 mul.214
  39.7 0.1 reshape.441
  39.8 0.8 mul.225
  40.6 0.1 mul.211
  40.6 0.8 mul.233
  41.4 0.1 reshape.464
  41.5 0.1 convert_reduce_fusion
  41.6 0.1 reshape.483
  41.7 0.1 reshape.442
  41.8 0.1 reshape.447
  41.9 0.1 multiply_reduce_fusion.2
  42.1 0.1 reshape.448
  42.1 0.1 fusion.45
  42.2 13.6 %fusion.48 = f32[7,32,1,64]{3,2,1,0:T(1,128)S(1)} fusion(f32[7,32,64,1]{2,3,1,0:T(1,128)S(1)} %bitcast.104, f32[7,32,64,64]{3,2,1,0:T(8,128)} %param.25), kind=kOutput, calls=%fused_computation.134 | convolution fusion | flops 11010048 | bytes 3784704 | tf_op jit(solution)/shard_map/bhvk,bhk->bhv/dot_general | solution.py:74
  55.9 7.9 %multiply_add_fusion = f32[7,32,64,64]{3,2,1,0:T(8,128)S(1)} fusion(f32[7,32,64,64]{3,2,1,0:T(8,128)} %param.25, f32[7,32,64]{2,1,0:T(8,128)S(1)} %get-tuple-element.15, f32[7,32,64]{2,1,0:T(8,128)S(1)} %reshape.448, f32[7,32,64]{2,1,0:T(8,128)S(1)} %get-tuple-element.13, f32[7,32,64]{2,1,0:T(8,128)S(1)} %bitcast.103, f32[7,32,64]{2,1,0:T(8,128)S(1)} %mul.211), kind=kLoop, calls=%fused_computation.2 | loop fusion | flops 4587520 | bytes 7626752 | tf_op jit(solution)/shard_map/add | solution.py:78
  63.8 3.0 %copy-done.1 = f32[7,32,64,64]{3,2,1,0:T(8,128)} copy-done((f32[7,32,64,64]{3,2,1,0:T(8,128)}, f32[7,32,64,64]{3,2,1,0:T(8,128)S(1)}, u32[]{:S(2)}) %copy-start.1) | copy-done | bytes 3670040
  66.9 5.8 %fusion.49 = f32[7,32,1,64]{3,2,1,0:T(1,128)S(1)} fusion(f32[7,32,64,64]{3,2,1,0:T(8,128)S(1)} %multiply_add_fusion, bf16[7,32,64,1]{2,3,1,0:T(2,128)(2,1)S(1)} %reshape.483), kind=kOutput, calls=%fused_computation.135 | convolution fusion | flops 11010048 | bytes 3756032 | tf_op jit(solution)/shard_map/bhvk,bhk->bhv/dot_general | solution.py:82
  72.7 0.1 reduce_sum.203
  72.8 0.2 multiply_reduce_fusion.1
  73.0 0.5 fusion.8
  73.5 0.1 reshape.475
  73.6 23.2 %all-gather.1 = bf16[16,7,2048]{2,1,0:T(8,128)(2,1)S(1)} all-gather(bf16[1,7,2048]{2,1,0:T(8,128)(2,1)S(1)} %reshape.475), channel_id=1, replica_groups=mesh['grp'=2,'ep'=16] {'ep'}, dimensions={0}, use_global_device_ids=true | all-gather | bytes 487424 | tf_op jit(solution)/shard_map/all_gather | solution.py:218
  96.8 0.2 reshape.476
  97.0 1.3 convolution_convert_fusion.2
  98.3 0.6 all_to_all.33
  98.9 3.5 %all-to-all-start.1 = ((bf16[16,7,128]{2,1,0:T(8,128)(2,1)}), bf16[16,7,128]{2,1,0:T(8,128)(2,1)S(1)}, u32[]{:S(2)}, u32[]{:S(2)}) async-start(bf16[16,7,128]{2,1,0:T(8,128)(2,1)} %all_to_all.33), calls=%async_computation.1 | async-start | bytes 65536 | tf_op jit(solution)/shard_map/all_to_all | solution.py:222
  102.4 6.6 %all-to-all-done.1 = bf16[16,7,128]{2,1,0:T(8,128)(2,1)S(1)} async-done(((bf16[16,7,128]{2,1,0:T(8,128)(2,1)}), bf16[16,7,128]{2,1,0:T(8,128)(2,1)S(1)}, u32[]{:S(2)}, u32[]{:S(2)}) %all-to-all-start.1) | async-done | bytes 28704 | tf_op jit(solution)/shard_map/all_to_all | solution.py:222
  109.0 0.1 fusion.26
  109.2 0.2 multiply_reduce_fusion.4
  109.4 0.1 multiply_convert_fusion.1
  109.5 0.2 fusion.50
  109.7 0.7 reshape.443
  110.4 3.5 %all-to-all-start.2 = ((bf16[16,2,2048]{2,1,0:T(2,128)(2,1)}), bf16[16,2,2048]{2,1,0:T(2,128)(2,1)S(1)}, u32[]{:S(2)}, u32[]{:S(2)}) async-start(bf16[16,2,2048]{2,1,0:T(2,128)(2,1)} %reshape.443), calls=%async_computation.2 | async-start | bytes 262144 | tf_op jit(solution)/shard_map/all_to_all | solution.py:150
  114.0 0.1 fusion.47
  114.2 0.3 select_reduce_fusion.4
  114.4 7.4 %all-to-all-done.2 = bf16[16,2,2048]{2,1,0:T(2,128)(2,1)S(1)} async-done(((bf16[16,2,2048]{2,1,0:T(2,128)(2,1)}), bf16[16,2,2048]{2,1,0:T(2,128)(2,1)S(1)}, u32[]{:S(2)}, u32[]{:S(2)}) %all-to-all-start.2) | async-done | bytes 131104 | tf_op jit(solution)/shard_map/all_to_all | solution.py:150
  121.8 0.1 reshape.444
  121.9 1.5 %fusion.17 = f32[32,256]{1,0:T(8,128)S(1)} fusion(bf16[32,2048]{1,0:T(8,128)(2,1)S(1)} %reshape.444, bf16[1,2048,256]{2,1,0:T(8,128)(2,1)} %param.43), kind=kOutput, calls=%fused_computation.29 | convolution fusion | flops 33554432 | bytes 1212416 | tf_op jit(solution)/shard_map/dot_general | solution.py:131
  123.4 0.0 copy-done
  123.4 0.7 convolution_convert_fusion
  124.1 0.8 reshape.445
  124.9 3.5 %all-to-all-start.3 = ((bf16[16,2,2048]{2,1,0:T(2,128)(2,1)}), bf16[16,2,2048]{2,1,0:T(2,128)(2,1)S(1)}, u32[]{:S(2)}, u32[]{:S(2)}) async-start(bf16[16,2,2048]{2,1,0:T(2,128)(2,1)} %reshape.445), calls=%async_computation.3 | async-start | bytes 262144 | tf_op jit(solution)/shard_map/all_to_all | solution.py:153
  128.5 0.1 copy.42
  128.6 7.7 %all-to-all-done.3 = bf16[16,2,2048]{2,1,0:T(2,128)(2,1)S(1)} async-done(((bf16[16,2,2048]{2,1,0:T(2,128)(2,1)}), bf16[16,2,2048]{2,1,0:T(2,128)(2,1)S(1)}, u32[]{:S(2)}, u32[]{:S(2)}) %all-to-all-start.3) | async-done | bytes 131104 | tf_op jit(solution)/shard_map/all_to_all | solution.py:153
  136.3 0.1 reshape.446
  136.3 0.6 gather_fusion
  137.0 0.1 reshape.472
  137.1 0.2 multiply_reduce_fusion
  137.3 0.1 fusion.32
  137.4 0.2 multiply_reduce_fusion.3
  137.6 0.7 multiply_convert_fusion
  (34 shorter events, 0.3 us)
Async XLA Ops:
  0.6 122.8 %copy-start = (bf16[1,256,2048]{2,1,0:T(8,128)(2,1)S(1)}, bf16[1,256,2048]{2,1,0:T(8,128)(2,1)}, u32[]{:S(2)}) copy-start(bf16[1,256,2048]{2,1,0:T(8,128)(2,1)} %param.45) | copy-start | bytes 3145732
  30.4 11.1 %all-to-all-start = ((bf16[112,3,128]{2,1,0:T(4,128)(2,1)}), bf16[112,3,128]{2,1,0:T(4,128)(2,1)S(1)}, u32[]{:S(2)}, u32[]{:S(2)}) async-start(bf16[112,3,128]{2,1,0:T(4,128)(2,1)} %copy.40), calls=%async_computation | async-start | bytes 229376 | tf_op jit(solution)/shard_map/all_to_all | solution.py:199
  63.8 3.1 %copy-start.1 = (f32[7,32,64,64]{3,2,1,0:T(8,128)}, f32[7,32,64,64]{3,2,1,0:T(8,128)S(1)}, u32[]{:S(2)}) copy-start(f32[7,32,64,64]{3,2,1,0:T(8,128)S(1)} %multiply_add_fusion) | copy-start | bytes 11010052
  66.8 6.2 %copy-start.4 = (f32[32,64]{1,0:T(8,128)S(1)}, f32[32,64]{1,0:T(8,128)}, u32[]{:S(2)}) copy-start(f32[32,64]{1,0:T(8,128)} %param.37) | copy-start | bytes 24580
  66.8 42.2 %copy-start.2 = (bf16[7,2048]{1,0:T(8,128)(2,1)S(1)}, bf16[7,2048]{1,0:T(8,128)(2,1)}, u32[]{:S(2)}) copy-start(bf16[7,2048]{1,0:T(8,128)(2,1)} %param.24) | copy-start | bytes 86020
  66.8 42.5 %copy-start.6 = (f32[2048]{0:T(1024)S(1)}, f32[2048]{0:T(1024)}, u32[]{:S(2)}) copy-start(f32[2048]{0:T(1024)} %param.40) | copy-start | bytes 24580
  66.8 47.1 %copy-start.8 = (bf16[2048,4]{0,1:T(4,128)(2,1)S(1)}, bf16[2048,4]{0,1:T(4,128)(2,1)}, u32[]{:S(2)}) copy-start(bf16[2048,4]{0,1:T(4,128)(2,1)} %param.41) | copy-start | bytes 49156
  66.8 47.3 %copy-start.7 = (bf16[2048,16]{0,1:T(8,128)(2,1)S(1)}, bf16[2048,16]{0,1:T(8,128)(2,1)}, u32[]{:S(2)}) copy-start(bf16[2048,16]{0,1:T(8,128)(2,1)} %param.42) | copy-start | bytes 196612
  66.9 56.5 %copy-start.3 = (bf16[1,2048,256]{2,1,0:T(8,128)(2,1)S(1)}, bf16[1,2048,256]{2,1,0:T(8,128)(2,1)}, u32[]{:S(2)}) copy-start(bf16[1,2048,256]{2,1,0:T(8,128)(2,1)} %param.44) | copy-start | bytes 3145732
  72.7 65.0 %copy-start.5 = (f32[2048]{0:T(1024)S(1)}, f32[2048]{0:T(1024)}, u32[]{:S(2)}) copy-start(f32[2048]{0:T(1024)} %param.46) | copy-start | bytes 24580
  98.9 10.1 %all-to-all-start.1 = ((bf16[16,7,128]{2,1,0:T(8,128)(2,1)}), bf16[16,7,128]{2,1,0:T(8,128)(2,1)S(1)}, u32[]{:S(2)}, u32[]{:S(2)}) async-start(bf16[16,7,128]{2,1,0:T(8,128)(2,1)} %all_to_all.33), calls=%async_computation.1 | async-start | bytes 65536 | tf_op jit(solution)/shard_map/all_to_all | solution.py:222
  110.4 11.4 %all-to-all-start.2 = ((bf16[16,2,2048]{2,1,0:T(2,128)(2,1)}), bf16[16,2,2048]{2,1,0:T(2,128)(2,1)S(1)}, u32[]{:S(2)}, u32[]{:S(2)}) async-start(bf16[16,2,2048]{2,1,0:T(2,128)(2,1)} %reshape.443), calls=%async_computation.2 | async-start | bytes 262144 | tf_op jit(solution)/shard_map/all_to_all | solution.py:150
  124.9 11.4 %all-to-all-start.3 = ((bf16[16,2,2048]{2,1,0:T(2,128)(2,1)}), bf16[16,2,2048]{2,1,0:T(2,128)(2,1)S(1)}, u32[]{:S(2)}, u32[]{:S(2)}) async-start(bf16[16,2,2048]{2,1,0:T(2,128)(2,1)} %reshape.445), calls=%async_computation.3 | async-start | bytes 262144 | tf_op jit(solution)/shard_map/all_to_all | solution.py:153
where the time goes:
time: 139 us; the launch traced here: 138 us
  blocking collectives  48.2 us (35%)
  matrix products  30.5 us (22%)
  waiting for transfers between devices  21.7 us (16%)
  starting transfers between devices  14 us (10%)
  other arithmetic  12 us (9%)
  local copies, waits for them, and re-layouts  11 us (8%)
    all_gather x1, blocking collectives, on_device(): section = lax.all_gather(sequence_input_rows, 'ep', axis=0, tiled=True)  25 us
    all_gather x1, blocking collectives, on_device(): lax.all_gather(attention_mixing_outcome, 'ep', axis=0, tiled=True)  23.2 us
    dot_general x1, matrix products, token_mixer_step(): jnp.einsum('bhvk,bhk->bhv', value_key_state, removal_dir, precision=lax.P...  13.6 us
    add x1, other arithmetic, token_mixer_step(): value_key_state * decay_heads[:, :, None, :]  7.89 us
    all_to_all x1, waiting for transfers between devices, by_exchange(): lax.all_to_all(finished, 'ep', split_axis=0, concat_axis=0, tiled=True)  7.72 us
    all_to_all x1, waiting for transfers between devices, by_exchange(): lax.all_to_all(outgoing, 'ep', split_axis=0, concat_axis=0, tiled=True)  7.39 us
    all_to_all x1, waiting for transfers between devices, on_device(): lax.all_to_all(out_columns, 'ep', split_axis=0, concat_axis=1, tiled=True)  6.58 us
    dot_general x1, matrix products, token_mixer_step(): jnp.einsum('bhvk,bhk->bhv', next_recurrent_state, acceptance_subspaces, p...  5.79 us
  transfers between devices with their start and end apart: 4, of which 3 were waited for; matrix products, arithmetic and copies ran while one was open for 6% of the time, Pallas kernels for 0%

commit v1 on v0

--- a/solution.py
+++ b/solution.py
@@ -219,7 +219,10 @@
         mixer_output_matrix,
         preferred_element_type=jnp.float32,
     ).astype(jnp.bfloat16)
-    attn_out = lax.all_to_all(out_columns, "ep", split_axis=0, concat_axis=1, tiled=True)
+    attn_out = jnp.concatenate(
+        lax.all_to_all(jnp.stack(jnp.split(out_columns, lax.axis_size("ep"), axis=0)), "ep", 0, 0),
+        axis=1,
+    )
     hidden = layer_norm(
         residual_scale * sequence_input_rows.astype(jnp.float32) + attn_out.astype(jnp.float32),
         mixer_norm_gain,

time: 139 us -> 148 us (1.065)
  local copies, waits for them, and re-layouts: 11 us -> 19.7 us
    unnamed x22 -> x37, local copies, waits for them, and re-layouts: 4.3 us -> 13 us
where the time goes in v1:
time: 148 us; the launch traced here: 147 us
  blocking collectives  48.2 us (33%)
  matrix products  30.5 us (21%)
  waiting for transfers between devices  21.7 us (15%)
  local copies, waits for them, and re-layouts  19.7 us (13%)
  starting transfers between devices  14.2 us (10%)
  other arithmetic  12 us (8%)
    all_gather x1, blocking collectives, on_device(): section = lax.all_gather(sequence_input_rows, 'ep', axis=0, tiled=True)  25 us
    all_gather x1, blocking collectives, on_device(): lax.all_gather(attention_mixing_outcome, 'ep', axis=0, tiled=True)  23.2 us
    dot_general x1, matrix products, token_mixer_step(): jnp.einsum('bhvk,bhk->bhv', value_key_state, removal_dir, precision=lax.P...  13.6 us
    unnamed x37, local copies, waits for them, and re-layouts  13 us
    add x1, other arithmetic, token_mixer_step(): value_key_state * decay_heads[:, :, None, :]  7.89 us
    all_to_all x1, waiting for transfers between devices, by_exchange(): lax.all_to_all(finished, 'ep', split_axis=0, concat_axis=0, tiled=True)  7.72 us
    all_to_all x1, waiting for transfers between devices, by_exchange(): lax.all_to_all(outgoing, 'ep', split_axis=0, concat_axis=0, tiled=True)  7.39 us
    all_to_all x1, waiting for transfers between devices, on_device(): lax.all_to_all(jnp.stack(jnp.split(out_columns, lax.axis_size('ep'), axis...  6.58 us
  transfers between devices with their start and end apart: 4, of which 3 were waited for; matrix products, arithmetic and copies ran while one was open for 6% of the time, Pallas kernels for 0%

profile of v1, /device:TPU:0, one launch (start us, length us, event | category | flops | bytes accessed | tf_op | source)
XLA Modules:
  0.0 147.2 jit_solution(13530235959871318910)
XLA Ops:
  0.6 25.0 %all-gather = bf16[16,7,2048]{2,1,0:T(8,128)(2,1)S(1)} all-gather(bf16[1,7,2048]{2,1,0:T(8,128)(2,1)} %bitcast.165), channel_id=1, replica_groups=mesh['grp'=2,'ep'=16] {'ep'}, dimensions={0}, use_global_device_ids=true | all-gather | bytes 487424 | tf_op jit(solution)/shard_map/all_gather | solution.py:193
  25.6 0.2 reshape.473
  25.8 1.3 fusion.10
  27.1 1.3 fusion.11
  28.4 1.3 fusion.9
  29.7 0.7 copy.40
  30.4 3.5 %all-to-all-start = ((bf16[112,3,128]{2,1,0:T(4,128)(2,1)}), bf16[112,3,128]{2,1,0:T(4,128)(2,1)S(1)}, u32[]{:S(2)}, u32[]{:S(2)}) async-start(bf16[112,3,128]{2,1,0:T(4,128)(2,1)} %copy.40), calls=%async_computation | async-start | bytes 229376 | tf_op jit(solution)/shard_map/all_to_all | solution.py:199
  34.0 0.8 copy.43
  34.9 0.3 select_reduce_fusion
  35.1 1.4 fusion.4
  36.6 1.5 %fusion.24 = f32[7,2048]{1,0:T(8,128)S(1)} fusion(bf16[64,2048]{1,0:T(8,128)(2,1)} %param.30, bf16[7,2048]{1,0:T(8,128)(2,1)} %param.24, bf16[2048,64]{0,1:T(8,128)(2,1)} %param.29, f32[2048]{0:T(1024)} %param.31), kind=kOutput, calls=%fused_computation.45 | convolution fusion | flops 3828160 | bytes 618496 | tf_op jit(solution)/shard_map/dot_general | solution.py:40
  38.1 0.8 slice_bitcast_fusion.18
  38.9 0.8 mul.214
  39.8 0.8 mul.225
  40.6 0.8 mul.233
  41.6 0.1 reshape.482
  41.9 0.1 multiply_reduce_fusion.2
  42.2 13.6 %fusion.48 = f32[7,32,1,64]{3,2,1,0:T(1,128)S(1)} fusion(f32[7,32,64,1]{2,3,1,0:T(1,128)S(1)} %bitcast.168, f32[7,32,64,64]{3,2,1,0:T(8,128)} %param.25), kind=kOutput, calls=%fused_computation.166 | convolution fusion | flops 11010048 | bytes 3784704 | tf_op jit(solution)/shard_map/bhvk,bhk->bhv/dot_general | solution.py:74
  55.9 7.9 %multiply_add_fusion = f32[7,32,64,64]{3,2,1,0:T(8,128)S(1)} fusion(f32[7,32,64,64]{3,2,1,0:T(8,128)} %param.25, f32[7,32,64]{2,1,0:T(8,128)S(1)} %get-tuple-element.15, f32[7,32,64]{2,1,0:T(8,128)S(1)} %reshape.447, f32[7,32,64]{2,1,0:T(8,128)S(1)} %get-tuple-element.13, f32[7,32,64]{2,1,0:T(8,128)S(1)} %bitcast.167, f32[7,32,64]{2,1,0:T(8,128)S(1)} %mul.211), kind=kLoop, calls=%fused_computation.2 | loop fusion | flops 4587520 | bytes 7626752 | tf_op jit(solution)/shard_map/add | solution.py:78
  63.8 3.0 %copy-done.1 = f32[7,32,64,64]{3,2,1,0:T(8,128)} copy-done((f32[7,32,64,64]{3,2,1,0:T(8,128)}, f32[7,32,64,64]{3,2,1,0:T(8,128)S(1)}, u32[]{:S(2)}) %copy-start.1) | copy-done | bytes 3670040
  66.9 5.8 %fusion.49 = f32[7,32,1,64]{3,2,1,0:T(1,128)S(1)} fusion(f32[7,32,64,64]{3,2,1,0:T(8,128)S(1)} %multiply_add_fusion, bf16[7,32,64,1]{2,3,1,0:T(2,128)(2,1)S(1)} %reshape.482), kind=kOutput, calls=%fused_computation.167 | convolution fusion | flops 11010048 | bytes 3756032 | tf_op jit(solution)/shard_map/bhvk,bhk->bhv/dot_general | solution.py:82
  72.7 0.1 reduce_sum.203
  72.8 0.2 multiply_reduce_fusion.1
  73.0 0.5 fusion.8
  73.5 0.1 reshape.474
  73.6 23.2 %all-gather.1 = bf16[16,7,2048]{2,1,0:T(8,128)(2,1)S(1)} all-gather(bf16[1,7,2048]{2,1,0:T(8,128)(2,1)S(1)} %reshape.474), channel_id=1, replica_groups=mesh['grp'=2,'ep'=16] {'ep'}, dimensions={0}, use_global_device_ids=true | all-gather | bytes 487424 | tf_op jit(solution)/shard_map/all_gather | solution.py:218
  96.8 0.2 reshape.475
  97.0 1.3 convolution_convert_fusion.2
  98.3 0.6 constant_dynamic-update-slice_fusion.15
  98.9 0.6 constant_dynamic-update-slice_fusion.14
  99.4 0.6 constant_dynamic-update-slice_fusion.13
  100.0 0.6 constant_dynamic-update-slice_fusion.12
  100.6 0.6 constant_dynamic-update-slice_fusion.11
  101.2 0.6 constant_dynamic-update-slice_fusion.10
  101.8 0.6 constant_dynamic-update-slice_fusion.9
  102.4 0.6 constant_dynamic-update-slice_fusion.8
  102.9 0.6 constant_dynamic-update-slice_fusion.7
  103.5 0.6 constant_dynamic-update-slice_fusion.6
  104.1 0.6 constant_dynamic-update-slice_fusion.5
  104.7 0.6 constant_dynamic-update-slice_fusion.4
  105.3 0.6 constant_dynamic-update-slice_fusion.3
  105.8 0.6 constant_dynamic-update-slice_fusion.2
  106.4 0.6 constant_dynamic-update-slice_fusion.1
  107.0 0.6 constant_dynamic-update-slice_fusion
  107.6 3.7 %all-to-all-start.1 = ((bf16[16,7,128]{2,1,0:T(8,128)(2,1)}), bf16[16,7,128]{2,1,0:T(8,128)(2,1)S(1)}, u32[]{:S(2)}, u32[]{:S(2)}) async-start(bf16[16,7,128]{2,1,0:T(8,128)(2,1)} %constant_dynamic-update-slice_fusion), calls=%async_computation.1 | async-start | bytes 65536 | tf_op jit(solution)/shard_map/all_to_all | solution.py:223
  111.3 6.6 %all-to-all-done.1 = bf16[16,7,128]{2,1,0:T(8,128)(2,1)S(1)} async-done(((bf16[16,7,128]{2,1,0:T(8,128)(2,1)}), bf16[16,7,128]{2,1,0:T(8,128)(2,1)S(1)}, u32[]{:S(2)}, u32[]{:S(2)}) %all-to-all-start.1) | async-done | bytes 28704 | tf_op jit(solution)/shard_map/all_to_all | solution.py:223
  117.9 0.1 fusion.26
  118.0 0.2 multiply_reduce_fusion.4
  118.3 0.2 fusion.50
  118.6 0.7 reshape.442
  119.3 3.5 %all-to-all-start.2 = ((bf16[16,2,2048]{2,1,0:T(2,128)(2,1)}), bf16[16,2,2048]{2,1,0:T(2,128)(2,1)S(1)}, u32[]{:S(2)}, u32[]{:S(2)}) async-start(bf16[16,2,2048]{2,1,0:T(2,128)(2,1)} %reshape.442), calls=%async_computation.2 | async-start | bytes 262144 | tf_op jit(solution)/shard_map/all_to_all | solution.py:150
  122.8 0.1 fusion.47
  123.0 0.3 select_reduce_fusion.4
  123.3 7.4 %all-to-all-done.2 = bf16[16,2,2048]{2,1,0:T(2,128)(2,1)S(1)} async-done(((bf16[16,2,2048]{2,1,0:T(2,128)(2,1)}), bf16[16,2,2048]{2,1,0:T(2,128)(2,1)S(1)}, u32[]{:S(2)}, u32[]{:S(2)}) %all-to-all-start.2) | async-done | bytes 131104 | tf_op jit(solution)/shard_map/all_to_all | solution.py:150
  130.7 1.5 %fusion.17 = f32[32,256]{1,0:T(8,128)S(1)} fusion(bf16[32,2048]{1,0:T(8,128)(2,1)S(1)} %reshape.443, bf16[1,2048,256]{2,1,0:T(8,128)(2,1)} %param.43), kind=kOutput, calls=%fused_computation.29 | convolution fusion | flops 33554432 | bytes 1212416 | tf_op jit(solution)/shard_map/dot_general | solution.py:131
  132.3 0.7 convolution_convert_fusion
  133.0 0.8 reshape.444
  133.8 3.5 %all-to-all-start.3 = ((bf16[16,2,2048]{2,1,0:T(2,128)(2,1)}), bf16[16,2,2048]{2,1,0:T(2,128)(2,1)S(1)}, u32[]{:S(2)}, u32[]{:S(2)}) async-start(bf16[16,2,2048]{2,1,0:T(2,128)(2,1)} %reshape.444), calls=%async_computation.3 | async-start | bytes 262144 | tf_op jit(solution)/shard_map/all_to_all | solution.py:153
  137.4 7.7 %all-to-all-done.3 = bf16[16,2,2048]{2,1,0:T(2,128)(2,1)S(1)} async-done(((bf16[16,2,2048]{2,1,0:T(2,128)(2,1)}), bf16[16,2,2048]{2,1,0:T(2,128)(2,1)S(1)}, u32[]{:S(2)}, u32[]{:S(2)}) %all-to-all-start.3) | async-done | bytes 131104 | tf_op jit(solution)/shard_map/all_to_all | solution.py:153
  145.2 0.6 gather_fusion
  145.9 0.2 multiply_reduce_fusion
  146.1 0.1 fusion.32
  146.3 0.2 multiply_reduce_fusion.3
  146.5 0.7 multiply_convert_fusion
  (49 shorter events, 1.4 us)
Async XLA Ops:
  0.6 131.6 %copy-start = (bf16[1,256,2048]{2,1,0:T(8,128)(2,1)S(1)}, bf16[1,256,2048]{2,1,0:T(8,128)(2,1)}, u32[]{:S(2)}) copy-start(bf16[1,256,2048]{2,1,0:T(8,128)(2,1)} %param.45) | copy-start | bytes 3145732
  30.4 11.1 %all-to-all-start = ((bf16[112,3,128]{2,1,0:T(4,128)(2,1)}), bf16[112,3,128]{2,1,0:T(4,128)(2,1)S(1)}, u32[]{:S(2)}, u32[]{:S(2)}) async-start(bf16[112,3,128]{2,1,0:T(4,128)(2,1)} %copy.40), calls=%async_computation | async-start | bytes 229376 | tf_op jit(solution)/shard_map/all_to_all | solution.py:199
  63.8 3.1 %copy-start.1 = (f32[7,32,64,64]{3,2,1,0:T(8,128)}, f32[7,32,64,64]{3,2,1,0:T(8,128)S(1)}, u32[]{:S(2)}) copy-start(f32[7,32,64,64]{3,2,1,0:T(8,128)S(1)} %multiply_add_fusion) | copy-start | bytes 11010052
  66.8 6.2 %copy-start.4 = (f32[32,64]{1,0:T(8,128)S(1)}, f32[32,64]{1,0:T(8,128)}, u32[]{:S(2)}) copy-start(f32[32,64]{1,0:T(8,128)} %param.37) | copy-start | bytes 24580
  66.8 51.0 %copy-start.2 = (bf16[7,2048]{1,0:T(8,128)(2,1)S(1)}, bf16[7,2048]{1,0:T(8,128)(2,1)}, u32[]{:S(2)}) copy-start(bf16[7,2048]{1,0:T(8,128)(2,1)} %param.24) | copy-start | bytes 86020
  66.8 51.4 %copy-start.6 = (f32[2048]{0:T(1024)S(1)}, f32[2048]{0:T(1024)}, u32[]{:S(2)}) copy-start(f32[2048]{0:T(1024)} %param.40) | copy-start | bytes 24580
  66.8 56.0 %copy-start.8 = (bf16[2048,4]{0,1:T(4,128)(2,1)S(1)}, bf16[2048,4]{0,1:T(4,128)(2,1)}, u32[]{:S(2)}) copy-start(bf16[2048,4]{0,1:T(4,128)(2,1)} %param.41) | copy-start | bytes 49156
  66.8 56.2 %copy-start.7 = (bf16[2048,16]{0,1:T(8,128)(2,1)S(1)}, bf16[2048,16]{0,1:T(8,128)(2,1)}, u32[]{:S(2)}) copy-start(bf16[2048,16]{0,1:T(8,128)(2,1)} %param.42) | copy-start | bytes 196612
  66.9 65.4 %copy-start.3 = (bf16[1,2048,256]{2,1,0:T(8,128)(2,1)S(1)}, bf16[1,2048,256]{2,1,0:T(8,128)(2,1)}, u32[]{:S(2)}) copy-start(bf16[1,2048,256]{2,1,0:T(8,128)(2,1)} %param.44) | copy-start | bytes 3145732
  72.7 73.8 %copy-start.5 = (f32[2048]{0:T(1024)S(1)}, f32[2048]{0:T(1024)}, u32[]{:S(2)}) copy-start(f32[2048]{0:T(1024)} %param.46) | copy-start | bytes 24580
  107.6 10.3 %all-to-all-start.1 = ((bf16[16,7,128]{2,1,0:T(8,128)(2,1)}), bf16[16,7,128]{2,1,0:T(8,128)(2,1)S(1)}, u32[]{:S(2)}, u32[]{:S(2)}) async-start(bf16[16,7,128]{2,1,0:T(8,128)(2,1)} %constant_dynamic-update-slice_fusion), calls=%async_computation.1 | async-start | bytes 65536 | tf_op jit(solution)/shard_map/all_to_all | solution.py:223
  119.3 11.4 %all-to-all-start.2 = ((bf16[16,2,2048]{2,1,0:T(2,128)(2,1)}), bf16[16,2,2048]{2,1,0:T(2,128)(2,1)S(1)}, u32[]{:S(2)}, u32[]{:S(2)}) async-start(bf16[16,2,2048]{2,1,0:T(2,128)(2,1)} %reshape.442), calls=%async_computation.2 | async-start | bytes 262144 | tf_op jit(solution)/shard_map/all_to_all | solution.py:150
  133.8 11.4 %all-to-all-start.3 = ((bf16[16,2,2048]{2,1,0:T(2,128)(2,1)}), bf16[16,2,2048]{2,1,0:T(2,128)(2,1)S(1)}, u32[]{:S(2)}, u32[]{:S(2)}) async-start(bf16[16,2,2048]{2,1,0:T(2,128)(2,1)} %reshape.444), calls=%async_computation.3 | async-start | bytes 262144 | tf_op jit(solution)/shard_map/all_to_all | solution.py:153
